TPU v7x, 32 devices: a whole 2x2x4 slice. The times are simulated.
32 devices in a mesh: grp: 2 (over y), fs: 4 (over z), tp: 4 (over x, core).
Axes of the slice: x: 2, y: 2, z: 4, core: 2. Of those that a mesh axis runs over, the one named last changes fastest.
Arguments:
- tokens: bfloat16 [2048, 2048], P(('grp', 'fs')), parts along dimension 0, may hold values from -6 to 6
- ffn_pre_gain: bfloat16 [2048], replicated, may hold values from 0.099609375 to 1.8984375
- gate_weight: bfloat16 [2048, 5632], P('fs', 'tp'), may hold values from -0.125 to 0.125
- up_weight: bfloat16 [2048, 5632], P('fs', 'tp'), may hold values from -0.125 to 0.125
- down_weight: bfloat16 [5632, 2048], P('tp', 'fs'), may hold values from -0.078125 to 0.078125
- ffn_post_gain: bfloat16 [2048], replicated, may hold values from 0.099609375 to 1.8984375
- mix_pre_gain: bfloat16 [2048], replicated, may hold values from 0.099609375 to 1.8984375
- mix_u_weight: bfloat16 [2048, 2048], P('fs', 'tp'), may hold values from -0.125 to 0.125
- mix_v_weight: bfloat16 [2048, 2048], P('fs', 'tp'), may hold values from -0.125 to 0.125
- spatial_gain: bfloat16 [2048], P('tp'), may hold values from 0.099609375 to 1.8984375
- spatial_weight: bfloat16 [16, 128, 128], P('tp'), may hold values from -0.5 to 0.5
- spatial_bias: bfloat16 [16, 128], P('tp'), may hold values from 0.099609375 to 1.8984375
- mix_out_weight: bfloat16 [2048, 2048], P('tp', 'fs'), may hold values from -0.125 to 0.125
- mix_post_gain: bfloat16 [2048], replicated, may hold values from 0.099609375 to 1.8984375
- late_pre_gain: bfloat16 [2048], replicated, may hold values from 0.099609375 to 1.8984375
- late_post_gain: bfloat16 [2048], replicated, may hold values from 0.099609375 to 1.8984375
Outputs:
- result: bfloat16 [2048, 2048], P(('grp', 'fs')), parts along dimension 0
There are 2 independent parts, one for each index of `grp`. A program takes and returns all parts, laid end to end along the dimension named above; an argument that names none is the same for every part. Nothing has to cross between parts.
All inputs are finite; a program needn't handle non-finite values.
Results may differ from a plain program's by a relative error of at most 0.019.
Values may be sent and summed in bfloat16 or wider, within the bound.
No kernel may reach another device: no remote copies, remote signals or barrier semaphores. Data moves between devices by JAX's collectives and lax.ppermute only.
A program may use at most 128 MiB of HBM per device.

v0:
```python
import jax
import jax.numpy as jnp
from jax import lax
from jax.sharding import PartitionSpec as P

GROUP_WIDTH = 128
BLOCK = 128


def row_norm(values, gain):
    scale = lax.rsqrt(jnp.mean(values * values, axis=-1, keepdims=True) + 1e-06)
    return values * scale * gain.astype(jnp.float32)


def reduce_partial(terms):
    return lax.psum(terms.astype(jnp.bfloat16), "tp").astype(jnp.float32)


def add_branch(stream, terms, gain, factor):
    total = reduce_partial(terms)
    return (stream.astype(jnp.float32) + factor * row_norm(total, gain)).astype(jnp.bfloat16)


def gated_hidden(normed, gate_full, up_full):
    gate = jnp.dot(normed, gate_full, preferred_element_type=jnp.float32)
    upper = jnp.dot(normed, up_full, preferred_element_type=jnp.float32)
    return (jax.nn.silu(gate) * upper).astype(jnp.bfloat16)


def spatial_mix(u_linear, v_linear, spatial_gain, spatial_weight, spatial_bias):
    count = u_linear.shape[0]
    gated_u = jax.nn.gelu(u_linear, approximate=False)
    gating_v = jax.nn.gelu(v_linear, approximate=False)
    groups = gating_v.shape[1] // GROUP_WIDTH
    grouped = gating_v.reshape(count, groups, GROUP_WIDTH)
    centred = grouped - jnp.mean(grouped, axis=-1, keepdims=True)
    vnorm = centred * lax.rsqrt(jnp.mean(centred * centred, axis=-1, keepdims=True) + 1e-05)
    vnorm = (vnorm * spatial_gain.astype(jnp.float32).reshape(groups, GROUP_WIDTH)).astype(
        jnp.bfloat16
    )
    blocks = vnorm.reshape(count // BLOCK, BLOCK, groups, GROUP_WIDTH)
    lower = jnp.tril(jnp.ones((BLOCK, BLOCK), dtype=bool))
    masked = jnp.where(lower[None], spatial_weight, jnp.zeros_like(spatial_weight))
    spatial = jnp.einsum("gts,nsgc->ntgc", masked, blocks, preferred_element_type=jnp.float32)
    spatial = spatial + spatial_bias.astype(jnp.float32).T[None, :, :, None]
    return (gated_u * spatial.reshape(count, groups * GROUP_WIDTH)).astype(jnp.bfloat16)


def shards(
    tokens,
    ffn_pre_gain,
    gate_weight,
    up_weight,
    down_weight,
    ffn_post_gain,
    mix_pre_gain,
    mix_u_weight,
    mix_v_weight,
    spatial_gain,
    spatial_weight,
    spatial_bias,
    mix_out_weight,
    mix_post_gain,
    late_pre_gain,
    late_post_gain,
):
    normed = row_norm(tokens.astype(jnp.float32), ffn_pre_gain).astype(jnp.bfloat16)
    gate_full, up_full = (
        lax.all_gather(gate_weight, "fs", axis=0, tiled=True),
        lax.all_gather(up_weight, "fs", axis=0, tiled=True),
    )
    down_full = lax.all_gather(down_weight, "fs", axis=1, tiled=True)
    hidden = gated_hidden(normed, gate_full, up_full)
    terms = jnp.dot(hidden, down_full, preferred_element_type=jnp.float32)
    first = add_branch(tokens, terms, ffn_post_gain, 0.5)
    normed = row_norm(first.astype(jnp.float32), mix_pre_gain).astype(jnp.bfloat16)
    u_full, v_full = (
        lax.all_gather(mix_u_weight, "fs", axis=0, tiled=True),
        lax.all_gather(mix_v_weight, "fs", axis=0, tiled=True),
    )
    u_linear = jnp.dot(normed, u_full, preferred_element_type=jnp.float32)
    v_linear = jnp.dot(normed, v_full, preferred_element_type=jnp.float32)
    mixed = spatial_mix(u_linear, v_linear, spatial_gain, spatial_weight, spatial_bias)
    out_full = lax.all_gather(mix_out_weight, "fs", axis=1, tiled=True)
    terms = jnp.dot(mixed, out_full, preferred_element_type=jnp.float32)
    second = add_branch(first, terms, mix_post_gain, 1.0)
    normed = row_norm(second.astype(jnp.float32), late_pre_gain).astype(jnp.bfloat16)
    hidden = gated_hidden(normed, gate_full, up_full)
    terms = jnp.dot(hidden, down_full, preferred_element_type=jnp.float32)
    return add_branch(second, terms, late_post_gain, 0.5)


def solution(mesh):
    in_specs = (
        P(("grp", "fs"), None),
        P(),
        P("fs", "tp"),
        P("fs", "tp"),
        P("tp", "fs"),
        P(),
        P(),
        P("fs", "tp"),
        P("fs", "tp"),
        P("tp"),
        P("tp", None, None),
        P("tp", None),
        P("tp", "fs"),
        P(),
        P(),
        P(),
    )
    out_specs = P(("grp", "fs"), None)
    return jax.shard_map(shards, mesh=mesh, in_specs=in_specs, out_specs=out_specs, check_vma=False)
```

profile of v0, /device:TPU:0, one launch (start us, length us, event | category | flops | bytes accessed | tf_op | source)
XLA Modules:
  0.0 620.2 jit_solution(5151979985591970159)
XLA Ops:
  6.5 0.7 all-gather.7.cloned.1.call-update
  7.3 0.7 all-gather.11.cloned.1.call-update
  8.1 0.7 all-gather.9.cloned.1.call-update
  8.8 0.3 fusion.10
  9.1 109.2 %all-gather.7.cloned.1.call-done = bf16[2048,1408]{1,0:T(8,128)(2,1)} async-done(((bf16[512,1408]{1,0:T(8,128)(2,1)}), bf16[2048,1408]{1,0:T(8,128)(2,1)}) %all-gather.7.cloned.1.call-update) | async-done | bytes 5767184 | tf_op jit(solution)/shard_map/all_gather | solution.py:69
  118.3 4.5 fusion.59
  122.8 102.0 %all-gather.11.cloned.1.call-done = bf16[1408,2048]{1,0:T(8,128)(2,1)} async-done(((bf16[1408,512]{1,0:T(8,128)(2,1)}), bf16[1408,2048]{1,0:T(8,128)(2,1)}) %all-gather.11.cloned.1.call-update) | async-done | bytes 5767184 | tf_op jit(solution)/shard_map/all_gather | solution.py:72
  224.9 106.6 %all-gather.9.cloned.1.call-done = bf16[2048,1408]{1,0:T(8,128)(2,1)} async-done(((bf16[512,1408]{1,0:T(8,128)(2,1)}), bf16[2048,1408]{1,0:T(8,128)(2,1)}) %all-gather.9.cloned.1.call-update) | async-done | bytes 5767184 | tf_op jit(solution)/shard_map/all_gather | solution.py:70
  331.4 8.9 %convolution_convert_fusion.2 = bf16[256,2048]{1,0:T(8,128)(2,1)} fusion(bf16[1408,2048]{1,0:T(8,128)(2,1)} %all-gather.11.cloned.1.call-done, bf16[2048,1408]{1,0:T(8,128)(2,1)} %all-gather.9.cloned.1.call-done, f32[256,1408]{1,0:T(8,128)S(1)} %fusion.59, bf16[256,2048]{1,0:T(8,128)(2,1)S(1)} %copy-done, f32[2048]{0:T(1024)S(1)} %convert_element_type.82, ...), kind=kOutput, calls=%fused_computation.21 | convolution fusion | flops 2957574144 | bytes 15082496 | tf_op jit(solution)/shard_map/dot_general | solution.py:74
  340.5 0.5 all-gather.15.cloned.1.call-update
  341.0 0.5 all-gather.13.cloned.1.call-update
  341.6 0.7 all-gather.17.cloned.1.call-update
  342.7 32.4 %all-reduce.4.cloned.1.call-done = bf16[256,2048]{1,0:T(8,128)(2,1)} async-done(((bf16[256,2048]{1,0:T(8,128)(2,1)}), bf16[256,2048]{1,0:T(8,128)(2,1)}) %all-reduce.4.cloned.1.call-update) | async-done | bytes 1048592 | tf_op jit(solution)/shard_map/psum | solution.py:16
  375.1 1.5 fusion.2
  376.6 2.0 fusion.14
  378.6 44.1 %all-gather.15.cloned.1.call-done = bf16[2048,512]{1,0:T(8,128)(2,1)} async-done(((bf16[512,512]{1,0:T(8,128)(2,1)}), bf16[2048,512]{1,0:T(8,128)(2,1)}) %all-gather.15.cloned.1.call-update) | async-done | bytes 2097168 | tf_op jit(solution)/shard_map/all_gather | solution.py:79
  422.7 3.4 fusion.28
  426.5 0.3 reduce_sum.75
  426.8 0.6 multiply_reduce_fusion
  427.9 0.3 fusion.22
  428.5 40.1 %all-gather.13.cloned.1.call-done = bf16[2048,512]{1,0:T(8,128)(2,1)} async-done(((bf16[512,512]{1,0:T(8,128)(2,1)}), bf16[2048,512]{1,0:T(8,128)(2,1)}) %all-gather.13.cloned.1.call-update) | async-done | bytes 2097168 | tf_op jit(solution)/shard_map/all_gather | solution.py:78
  468.6 46.1 %all-gather.17.cloned.1.call-done = bf16[512,2048]{1,0:T(8,128)(2,1)} async-done(((bf16[512,512]{1,0:T(8,128)(2,1)}), bf16[512,2048]{1,0:T(8,128)(2,1)}) %all-gather.17.cloned.1.call-update) | async-done | bytes 2097168 | tf_op jit(solution)/shard_map/all_gather | solution.py:84
  514.7 5.7 convolution_convert_fusion
  520.4 0.3 all-reduce.8.cloned.1.call-start
  520.7 34.9 %all-reduce.6.cloned.1.call-done = bf16[256,2048]{1,0:T(8,128)(2,1)} async-done(((bf16[256,2048]{1,0:T(8,128)(2,1)}), bf16[256,2048]{1,0:T(8,128)(2,1)}) %all-reduce.6.cloned.1.call-update) | async-done | bytes 1048592 | tf_op jit(solution)/shard_map/psum | solution.py:16
  555.7 1.5 fusion.5
  557.2 1.9 fusion.18
  559.1 4.5 fusion.45
  563.6 8.9 %convolution_convert_fusion.1 = bf16[256,2048]{1,0:T(8,128)(2,1)} fusion(bf16[1408,2048]{1,0:T(8,128)(2,1)} %all-gather.11.cloned.1.call-done, bf16[2048,1408]{1,0:T(8,128)(2,1)} %all-gather.9.cloned.1.call-done, f32[256,1408]{1,0:T(8,128)S(1)} %fusion.45, bf16[256,2048]{1,0:T(8,128)(2,1)S(1)} %get-tuple-element.6, f32[2048]{0:T(1024)S(1)} %convert_element_type.99, ...), kind=kOutput, calls=%fused_computation.20 | convolution fusion | flops 2957574144 | bytes 15082496 | tf_op jit(solution)/shard_map/dot_general | solution.py:89
  572.5 36.9 %all-reduce.8.cloned.1.call-done = bf16[256,2048]{1,0:T(8,128)(2,1)} async-done(((bf16[256,2048]{1,0:T(8,128)(2,1)}), bf16[256,2048]{1,0:T(8,128)(2,1)}) %all-reduce.8.cloned.1.call-update) | async-done | bytes 1048592 | tf_op jit(solution)/shard_map/psum | solution.py:16
  609.4 1.5 fusion.7
  610.9 2.8 fusion.21
  (54 shorter events, 1.7 us)
Async XLA Ops:
  6.5 2.3 copy-start.2
  6.5 2.3 copy-start
  6.5 111.8 %all-gather.7.cloned.1.call-start = ((), (), s32[]{:S(2)}) async-start(), calls=%async_computation | async-start | bytes 7208960 | tf_op jit(solution)/shard_map/all_gather | solution.py:69
  7.3 217.6 %all-gather.11.cloned.1.call-start = ((), (), s32[]{:S(2)}) async-start(), calls=%async_computation.2 | async-start | bytes 7208960 | tf_op jit(solution)/shard_map/all_gather | solution.py:72
  8.0 323.4 %all-gather.9.cloned.1.call-start = ((), (), s32[]{:S(2)}) async-start(), calls=%async_computation.1 | async-start | bytes 7208960 | tf_op jit(solution)/shard_map/all_gather | solution.py:70
  8.7 366.4 %all-reduce.4.cloned.1.call-start = ((), (), s32[]{:S(2)}) async-start(), calls=%async_computation.3 | async-start | bytes 2097152 | tf_op jit(solution)/shard_map/psum | solution.py:16
  340.4 2.2 copy-start.3
  340.4 2.2 copy-start.4
  340.4 2.2 copy-start.8
  340.4 2.3 copy-start.9
  340.4 82.3 %all-gather.15.cloned.1.call-start = ((), (), s32[]{:S(2)}) async-start(), calls=%async_computation.5 | async-start | bytes 2621440 | tf_op jit(solution)/shard_map/all_gather | solution.py:79
  341.0 127.6 %all-gather.13.cloned.1.call-start = ((), (), s32[]{:S(2)}) async-start(), calls=%async_computation.4 | async-start | bytes 2621440 | tf_op jit(solution)/shard_map/all_gather | solution.py:78
  341.6 173.1 %all-gather.17.cloned.1.call-start = ((), (), s32[]{:S(2)}) async-start(), calls=%async_computation.6 | async-start | bytes 2621440 | tf_op jit(solution)/shard_map/all_gather | solution.py:84
  342.3 213.3 %all-reduce.6.cloned.1.call-start = ((), (), s32[]{:S(2)}) async-start(), calls=%async_computation.7 | async-start | bytes 2097152 | tf_op jit(solution)/shard_map/psum | solution.py:16
  426.3 1.7 copy-start.1
  514.7 6.0 copy-start.5
  514.7 6.0 copy-start.6
  520.4 89.0 %all-reduce.8.cloned.1.call-start = ((), (), s32[]{:S(2)}) async-start(), calls=%async_computation.8 | async-start | bytes 2097152 | tf_op jit(solution)/shard_map/psum | solution.py:16
  563.6 9.0 %copy-start.7 = (bf16[2048]{0:T(1024)(128)(2,1)S(1)}, bf16[2048]{0:T(1024)(128)(2,1)}, u32[]{:S(2)}) copy-start(bf16[2048]{0:T(1024)(128)(2,1)} %param.31) | copy-start | bytes 12292
Sparse Core Ops, SparseCore 0:
  8.9 109.3 all-gather.6
  119.9 104.9 all-gather.10
  226.5 104.9 all-gather.8
  340.5 34.5 all-reduce.3
  376.5 46.1 all-gather.14
  424.1 44.4 all-gather.12
  470.2 44.4 all-gather.16
  520.5 35.0 all-reduce.5
  572.6 36.7 all-reduce.7
where the time goes:
time: 621 us; the launch traced here: 620 us
  waiting for transfers between devices  556 us (90%)
  matrix products  36.2 us (6%)
  between operations  13.5 us (2%)
  other arithmetic  12.6 us (2%)
    all_gather x1, waiting for transfers between devices, shards(): lax.all_gather(gate_weight, 'fs', axis=0, tiled=True)  109 us
    all_gather x1, waiting for transfers between devices, shards(): lax.all_gather(up_weight, 'fs', axis=0, tiled=True)  107 us
    psum x3, waiting for transfers between devices, reduce_partial(): return lax.psum(terms.astype(jnp.bfloat16), 'tp').astype(jnp.float32)  104 us
    all_gather x1, waiting for transfers between devices, shards(): down_full = lax.all_gather(down_weight, 'fs', axis=1, tiled=True)  102 us
    all_gather x1, waiting for transfers between devices, shards(): out_full = lax.all_gather(mix_out_weight, 'fs', axis=1, tiled=True)  46.1 us
    all_gather x1, waiting for transfers between devices, shards(): lax.all_gather(mix_v_weight, 'fs', axis=0, tiled=True)  44.1 us
    all_gather x1, waiting for transfers between devices, shards(): lax.all_gather(mix_u_weight, 'fs', axis=0, tiled=True)  40.1 us
    dot_general x2, matrix products, shards(): terms = jnp.dot(hidden, down_full, preferred_element_type=jnp.float32)  17.8 us
  transfers between devices with their start and end apart: 9, of which 9 were waited for; matrix products, arithmetic and copies ran while one was open for 2% of the time, Pallas kernels for 0%

commit v1 on v0

--- a/solution.py
+++ b/solution.py
@@ -76,7 +76,9 @@
     normed = row_norm(first.astype(jnp.float32), mix_pre_gain).astype(jnp.bfloat16)
     u_full, v_full = (
         lax.all_gather(mix_u_weight, "fs", axis=0, tiled=True),
-        lax.all_gather(mix_v_weight, "fs", axis=0, tiled=True),
+        jnp.concatenate(
+            lax.all_to_all(jnp.stack([mix_v_weight] * lax.axis_size("fs")), "fs", 0, 0), axis=0
+        ),
     )
     u_linear = jnp.dot(normed, u_full, preferred_element_type=jnp.float32)
     v_linear = jnp.dot(normed, v_full, preferred_element_type=jnp.float32)

time: 621 us -> 582 us (0.937)
  waiting for transfers between devices: 556 us -> 512 us
    all_gather x1 -> x0, waiting for transfers between devices: 44.1 us -> none  [shards(): lax.all_gather(mix_v_weight, 'fs', axis=0, tiled=True)]
    all_to_all x0 -> x1, waiting for transfers between devices: none -> 37.9 us  [shards(): lax.all_to_all(jnp.stack([mix_v_weight] * lax.axis_size('fs')), 'fs', 0, 0)]
    all_gather x1, waiting for transfers between devices: 40.1 us -> 7.48 us  [shards(): lax.all_gather(mix_u_weight, 'fs', axis=0, tiled=True)]
  transfers between devices with their start and end apart: 9 -> 9, of which waited for: 9 -> 9; matrix products, arithmetic and copies ran while one was open for 2% -> 3% of each run, Pallas kernels for 0% -> 0%
where the time goes in v1:
time: 582 us
  waiting for transfers between devices  512 us (88%)
  matrix products  36.2 us (6%)
  between operations  13.8 us (2%)
  other arithmetic  12.5 us (2%)
    all_gather x1, waiting for transfers between devices, shards(): lax.all_gather(gate_weight, 'fs', axis=0, tiled=True)  109 us
    all_gather x1, waiting for transfers between devices, shards(): lax.all_gather(up_weight, 'fs', axis=0, tiled=True)  107 us
    all_gather x1, waiting for transfers between devices, shards(): down_full = lax.all_gather(down_weight, 'fs', axis=1, tiled=True)  102 us
    psum x3, waiting for transfers between devices, reduce_partial(): return lax.psum(terms.astype(jnp.bfloat16), 'tp').astype(jnp.float32)  99.1 us
    all_gather x1, waiting for transfers between devices, shards(): out_full = lax.all_gather(mix_out_weight, 'fs', axis=1, tiled=True)  46.1 us
    all_to_all x1, waiting for transfers between devices, shards(): lax.all_to_all(jnp.stack([mix_v_weight] * lax.axis_size('fs')), 'fs', 0, 0)  37.9 us
    dot_general x2, matrix products, shards(): terms = jnp.dot(hidden, down_full, preferred_element_type=jnp.float32)  17.8 us
  transfers between devices with their start and end apart: 9, of which 9 were waited for; matrix products, arithmetic and copies ran while one was open for 3% of the time, Pallas kernels for 0%

profile of v1, /device:TPU:0, one launch (start us, length us, event | category | flops | bytes accessed | tf_op | source)
XLA Modules:
  0.0 581.9 jit_solution(1028414234146191270)
XLA Ops:
  6.5 0.7 all-gather.6.cloned.1.call-update
  7.3 0.7 all-gather.10.cloned.1.call-update
  8.1 0.7 all-gather.8.cloned.1.call-update
  8.8 0.3 fusion.10
  9.1 109.2 %all-gather.6.cloned.1.call-done = bf16[2048,1408]{1,0:T(8,128)(2,1)} async-done(((bf16[512,1408]{1,0:T(8,128)(2,1)}), bf16[2048,1408]{1,0:T(8,128)(2,1)}) %all-gather.6.cloned.1.call-update) | async-done | bytes 5767184 | tf_op jit(solution)/shard_map/all_gather | solution.py:69
  118.3 4.5 fusion.59
  122.8 102.0 %all-gather.10.cloned.1.call-done = bf16[1408,2048]{1,0:T(8,128)(2,1)} async-done(((bf16[1408,512]{1,0:T(8,128)(2,1)}), bf16[1408,2048]{1,0:T(8,128)(2,1)}) %all-gather.10.cloned.1.call-update) | async-done | bytes 5767184 | tf_op jit(solution)/shard_map/all_gather | solution.py:72
  224.9 106.6 %all-gather.8.cloned.1.call-done = bf16[2048,1408]{1,0:T(8,128)(2,1)} async-done(((bf16[512,1408]{1,0:T(8,128)(2,1)}), bf16[2048,1408]{1,0:T(8,128)(2,1)}) %all-gather.8.cloned.1.call-update) | async-done | bytes 5767184 | tf_op jit(solution)/shard_map/all_gather | solution.py:70
  331.4 8.9 %convolution_convert_fusion.2 = bf16[256,2048]{1,0:T(8,128)(2,1)} fusion(bf16[1408,2048]{1,0:T(8,128)(2,1)} %all-gather.10.cloned.1.call-done, bf16[2048,1408]{1,0:T(8,128)(2,1)} %all-gather.8.cloned.1.call-done, f32[256,1408]{1,0:T(8,128)S(1)} %fusion.59, bf16[256,2048]{1,0:T(8,128)(2,1)S(1)} %copy-done, f32[2048]{0:T(1024)S(1)} %convert_element_type.82, ...), kind=kOutput, calls=%fused_computation.21 | convolution fusion | flops 2957574144 | bytes 15082496 | tf_op jit(solution)/shard_map/dot_general | solution.py:74
  340.4 0.5 all-gather.12.cloned.1.call-update
  341.0 1.6 stack.2
  342.6 4.6 all-to-all-start
  347.2 0.5 all-gather.14.cloned.1.call-update
  348.1 27.3 %all-reduce.4.cloned.1.call-done = bf16[256,2048]{1,0:T(8,128)(2,1)} async-done(((bf16[256,2048]{1,0:T(8,128)(2,1)}), bf16[256,2048]{1,0:T(8,128)(2,1)}) %all-reduce.4.cloned.1.call-update) | async-done | bytes 1048592 | tf_op jit(solution)/shard_map/psum | solution.py:16
  375.4 1.5 fusion.2
  376.9 2.0 fusion.14
  378.8 37.9 %all-to-all-done = bf16[4,512,512]{2,1,0:T(8,128)(2,1)} async-done(((bf16[4,512,512]{2,1,0:T(8,128)(2,1)}), bf16[4,512,512]{2,1,0:T(8,128)(2,1)}, u32[]{:S(2)}, u32[]{:S(2)}) %all-to-all-start) | async-done | bytes 2097184 | tf_op jit(solution)/shard_map/all_to_all | solution.py:80
  416.7 3.4 fusion.28
  420.5 0.3 reduce_sum.75
  420.8 0.6 multiply_reduce_fusion
  421.9 0.3 fusion.22
  422.5 7.5 %all-gather.12.cloned.1.call-done = bf16[2048,512]{1,0:T(8,128)(2,1)} async-done(((bf16[512,512]{1,0:T(8,128)(2,1)}), bf16[2048,512]{1,0:T(8,128)(2,1)}) %all-gather.12.cloned.1.call-update) | async-done | bytes 2097168 | tf_op jit(solution)/shard_map/all_gather | solution.py:78
  430.0 46.1 %all-gather.14.cloned.1.call-done = bf16[512,2048]{1,0:T(8,128)(2,1)} async-done(((bf16[512,512]{1,0:T(8,128)(2,1)}), bf16[512,2048]{1,0:T(8,128)(2,1)}) %all-gather.14.cloned.1.call-update) | async-done | bytes 2097168 | tf_op jit(solution)/shard_map/all_gather | solution.py:86
  476.0 5.7 convolution_convert_fusion
  482.1 34.9 %all-reduce.6.cloned.1.call-done = bf16[256,2048]{1,0:T(8,128)(2,1)} async-done(((bf16[256,2048]{1,0:T(8,128)(2,1)}), bf16[256,2048]{1,0:T(8,128)(2,1)}) %all-reduce.6.cloned.1.call-update) | async-done | bytes 1048592 | tf_op jit(solution)/shard_map/psum | solution.py:16
  517.0 1.5 fusion.5
  518.5 1.9 fusion.18
  520.4 4.5 fusion.45
  524.9 8.9 %convolution_convert_fusion.1 = bf16[256,2048]{1,0:T(8,128)(2,1)} fusion(bf16[1408,2048]{1,0:T(8,128)(2,1)} %all-gather.10.cloned.1.call-done, bf16[2048,1408]{1,0:T(8,128)(2,1)} %all-gather.8.cloned.1.call-done, f32[256,1408]{1,0:T(8,128)S(1)} %fusion.45, bf16[256,2048]{1,0:T(8,128)(2,1)S(1)} %get-tuple-element.6, f32[2048]{0:T(1024)S(1)} %convert_element_type.99, ...), kind=kOutput, calls=%fused_computation.20 | convolution fusion | flops 2957574144 | bytes 15082496 | tf_op jit(solution)/shard_map/dot_general | solution.py:91
  533.9 36.9 %all-reduce.8.cloned.1.call-done = bf16[256,2048]{1,0:T(8,128)(2,1)} async-done(((bf16[256,2048]{1,0:T(8,128)(2,1)}), bf16[256,2048]{1,0:T(8,128)(2,1)}) %all-reduce.8.cloned.1.call-update) | async-done | bytes 1048592 | tf_op jit(solution)/shard_map/psum | solution.py:16
  570.8 1.5 fusion.7
  572.3 2.8 fusion.21
  (56 shorter events, 1.9 us)
Async XLA Ops:
  6.5 2.3 copy-start.3
  6.5 2.3 copy-start
  6.5 111.8 %all-gather.6.cloned.1.call-start = ((), (), s32[]{:S(2)}) async-start(), calls=%async_computation.1 | async-start | bytes 7208960 | tf_op jit(solution)/shard_map/all_gather | solution.py:69
  7.3 217.6 %all-gather.10.cloned.1.call-start = ((), (), s32[]{:S(2)}) async-start(), calls=%async_computation.3 | async-start | bytes 7208960 | tf_op jit(solution)/shard_map/all_gather | solution.py:72
  8.0 323.4 %all-gather.8.cloned.1.call-start = ((), (), s32[]{:S(2)}) async-start(), calls=%async_computation.2 | async-start | bytes 7208960 | tf_op jit(solution)/shard_map/all_gather | solution.py:70
  8.7 366.6 %all-reduce.4.cloned.1.call-start = ((), (), s32[]{:S(2)}) async-start(), calls=%async_computation.4 | async-start | bytes 2097152 | tf_op jit(solution)/shard_map/psum | solution.py:16
  122.8 218.2 %copy-start.1 = (bf16[512,512]{1,0:T(8,128)(2,1)S(1)}, bf16[512,512]{1,0:T(8,128)(2,1)}, u32[]{:S(2)}) copy-start(bf16[512,512]{1,0:T(8,128)(2,1)} %param.24) | copy-start | bytes 1572868
  340.4 89.6 %all-gather.12.cloned.1.call-start = ((), (), s32[]{:S(2)}) async-start(), calls=%async_computation.5 | async-start | bytes 2621440 | tf_op jit(solution)/shard_map/all_gather | solution.py:78
  342.6 5.4 copy-start.4
  342.6 5.4 copy-start.5
  342.6 5.5 copy-start.9
  342.6 5.5 copy-start.10
  342.6 74.1 %all-to-all-start = ((bf16[4,512,512]{2,1,0:T(8,128)(2,1)}), bf16[4,512,512]{2,1,0:T(8,128)(2,1)}, u32[]{:S(2)}, u32[]{:S(2)}) async-start(bf16[4,512,512]{2,1,0:T(8,128)(2,1)} %stack.2), calls=%async_computation | async-start | bytes 4194304 | tf_op jit(solution)/shard_map/all_to_all | solution.py:80
  347.2 128.8 %all-gather.14.cloned.1.call-start = ((), (), s32[]{:S(2)}) async-start(), calls=%async_computation.6 | async-start | bytes 2621440 | tf_op jit(solution)/shard_map/all_gather | solution.py:86
  347.8 169.3 %all-reduce.6.cloned.1.call-start = ((), (), s32[]{:S(2)}) async-start(), calls=%async_computation.7 | async-start | bytes 2097152 | tf_op jit(solution)/shard_map/psum | solution.py:16
  420.3 1.7 copy-start.2
  476.0 6.0 %copy-start.6 = (bf16[2048]{0:T(1024)(128)(2,1)S(1)}, bf16[2048]{0:T(1024)(128)(2,1)}, u32[]{:S(2)}) copy-start(bf16[2048]{0:T(1024)(128)(2,1)} %param.29) | copy-start | bytes 12292
  476.0 6.0 %copy-start.7 = (bf16[2048]{0:T(1024)(128)(2,1)S(1)}, bf16[2048]{0:T(1024)(128)(2,1)}, u32[]{:S(2)}) copy-start(bf16[2048]{0:T(1024)(128)(2,1)} %param.30) | copy-start | bytes 12292
  481.7 89.0 %all-reduce.8.cloned.1.call-start = ((), (), s32[]{:S(2)}) async-start(), calls=%async_computation.8 | async-start | bytes 2097152 | tf_op jit(solution)/shard_map/psum | solution.py:16
  524.9 9.0 %copy-start.8 = (bf16[2048]{0:T(1024)(128)(2,1)S(1)}, bf16[2048]{0:T(1024)(128)(2,1)}, u32[]{:S(2)}) copy-start(bf16[2048]{0:T(1024)(128)(2,1)} %param.31) | copy-start | bytes 12292
Sparse Core Ops, SparseCore 0:
  8.9 109.3 all-gather.5
  119.9 104.9 all-gather.9
  226.5 104.9 all-gather.7
  340.5 34.7 all-reduce.3
  376.8 53.1 all-gather.11
  431.4 44.5 all-gather.13
  481.9 35.0 all-reduce.5
  534.0 36.7 all-reduce.7
